TPU v7x, 32 devices: a whole 2x2x4 slice. The times are simulated.
32 devices in a mesh: sp: 16 (over z, y, x), tp: 2 (over core).
Axes of the slice: x: 2, y: 2, z: 4, core: 2. Of those that a mesh axis runs over, the one named last changes fastest.
Arguments:
- prompt: bfloat16 [1, 8192, 2048], P(None, 'sp', 'tp'), may hold values from -6 to 6
- new_token: bfloat16 [1, 2048], P(None, 'tp'), may hold values from -6 to 6
- w_query: bfloat16 [2048, 2048], P(None, 'tp'), may hold values from -0.125 to 0.125
- w_key: bfloat16 [2048, 2048], P(None, 'tp'), may hold values from -0.125 to 0.125
- w_value: bfloat16 [2048, 2048], P(None, 'tp'), may hold values from -0.125 to 0.125
- decay_rate: float32 [16], P('tp'), may hold values from 1e-05 to 0.06
- norm_gain: float32 [2048], P('tp'), may hold values from 0.1 to 1.9
Outputs:
- mixed: bfloat16 [1, 8192, 2048], P(None, 'sp', 'tp')
- cache: bfloat16 [1, 16, 128, 128], P(None, 'tp', 'sp')
- new_read: bfloat16 [1, 2048], P(None, 'tp')
All inputs are finite; a program needn't handle non-finite values.
Results may differ from a plain program's by a relative error of at most 0.0083.
Values may be sent and summed in bfloat16 or wider, within the bound.
A program may use at most 64 MiB of HBM per device.

v0:
```python
import functools

import jax
import jax.numpy as jnp
import numpy as np
from jax import lax
from jax.experimental import pallas as pl
from jax.experimental.pallas import tpu as pltpu
from jax.sharding import PartitionSpec as P

HEAD = 128
PAD = 16
rope_base = 10000.0
norm_floor = 1e-05
MESH = pl.DeviceIdType.MESH
BF = jnp.bfloat16
F32 = jnp.float32


def head_norm(o, gain):
    center = jnp.mean(o, axis=-1, keepdims=True)
    delta = o - center
    spread = jnp.mean(delta * delta, axis=-1, keepdims=True)
    return delta * lax.rsqrt(spread + norm_floor) * gain


def split(members):
    best = 1
    for g in range(1, members + 1):
        if members % g == 0 and g * g <= members:
            best = g
    return best


def dot(a, b):
    return jnp.dot(a, b, preferred_element_type=F32)


def kernel(cfg, x_hbm, tok_hbm, wq, wk, wv, rate, gain, tab_hbm, base, mixed, cache, read_out,
           xbuf, tokbuf, wbuf, acc, tab, ctab, stab, kbuf, qbuf, vbuf, intra, obuf,
           send1, recv1, pre, recv2, send3, recv3, pacc, fin, tokq, tokk, tokv, rdbuf,
           w_sem, l_sem, tps, tpr, s1s, s1r, s2s, s2r, s3s, s3r, rds, rdr, o_sem):
    M, G, Z, T, B, F, H, hc, R = cfg
    NC = H // hc
    W = hc * HEAD
    rank = lax.axis_index("sp")
    me = lax.axis_index("tp")
    z = rank // G
    j = rank % G
    weights = (wk, wv, wq)

    lx = pltpu.make_async_copy(x_hbm, xbuf.at[me, pl.ds(0, B)], l_sem.at[0])
    lt = pltpu.make_async_copy(tok_hbm, tokbuf.at[me], l_sem.at[1])
    ltab = pltpu.make_async_copy(tab_hbm, tab, l_sem.at[2])
    lx.start()
    lt.start()

    def wcopy(m, c, d):
        p = lax.rem(me + d, T)
        return pltpu.make_async_copy(
            weights[m].at[pl.ds(pl.multiple_of(p * F, HEAD), F), pl.ds(c * W, W)],
            wbuf.at[m, c, d], w_sem.at[m, c, d])

    for c in range(NC):
        wcopy(0, c, 0).start()
        wcopy(1, c, 0).start()
        if c == 0:
            ltab.start()
    for c in range(NC):
        for d in range(1, T):
            wcopy(0, c, d).start()
            wcopy(1, c, d).start()
    for c in range(NC):
        for d in range(T):
            wcopy(2, c, d).start()

    barrier = pltpu.get_barrier_semaphore()
    for d in range(1, T):
        pl.semaphore_signal(barrier, inc=1, device_id={"tp": lax.rem(me + d, T)}, device_id_type=MESH)
    for d in range(1, M):
        pl.semaphore_signal(barrier, inc=1, device_id={"sp": lax.rem(rank + d, M)}, device_id_type=MESH)

    def widen(p):
        t = tokbuf[p].astype(F32)
        xbuf[p, B:B + PAD, :] = jnp.broadcast_to(t, (PAD, F)).astype(BF)

    lt.wait()
    widen(me)
    lx.wait()

    def own_part(c):
        for m in range(2):
            wcopy(m, c, 0).wait()
            acc[m, c] = dot(xbuf[me], wbuf[m, c, 0])

    own_part(0)
    pl.semaphore_wait(barrier, T - 1 + M - 1)
    sends = []
    for d in range(1, T):
        peer = lax.rem(me + d, T)
        a = pltpu.make_async_remote_copy(
            src_ref=x_hbm, dst_ref=xbuf.at[me, pl.ds(0, B)], send_sem=tps.at[0, d],
            recv_sem=tpr.at[0, d], device_id={"tp": peer}, device_id_type=MESH)
        b = pltpu.make_async_remote_copy(
            src_ref=tok_hbm, dst_ref=tokbuf.at[me], send_sem=tps.at[1, d],
            recv_sem=tpr.at[1, d], device_id={"tp": peer}, device_id_type=MESH)
        a.start()
        b.start()
        sends += [a, b]

    ltab.wait()
    cb = base[rank, 0:1, :]
    sb = base[rank, 1:2, :]
    ctab[0:B, :] = cb * tab[0] - sb * tab[1]
    stab[0:B, :] = sb * tab[0] + cb * tab[1]
    ctab[B:B + PAD, :] = jnp.broadcast_to(base[M, 0:1, :], (PAD, HEAD))
    stab[B:B + PAD, :] = jnp.broadcast_to(base[M, 1:2, :], (PAD, HEAD))

    for c in range(1, NC):
        own_part(c)

    for d in range(1, T):
        src = lax.rem(me + T - d, T)
        pltpu.make_async_remote_copy(
            src_ref=tok_hbm, dst_ref=tokbuf.at[src], send_sem=tps.at[1, d],
            recv_sem=tpr.at[1, d], device_id={"tp": src}, device_id_type=MESH).wait_recv()
        pltpu.make_async_remote_copy(
            src_ref=x_hbm, dst_ref=xbuf.at[src, pl.ds(0, B)], send_sem=tps.at[0, d],
            recv_sem=tpr.at[0, d], device_id={"tp": src}, device_id_type=MESH).wait_recv()
        widen(src)

    def rotated(u):
        return u * ctab[...] + pltpu.roll(u, HEAD // 2, 1) * stab[...]

    def rest(m, c, total):
        for d in range(1, T):
            wcopy(m, c, d).wait()
            part = dot(xbuf[lax.rem(me + d, T)], wbuf[m, c, d])
            total = part if total is None else total + part
        return total

    steps = (lax.broadcasted_iota(jnp.int32, (B, HEAD), 0) + 1).astype(F32)

    def block_decay(c, power):
        rows = [jnp.exp(jnp.full((R, HEAD), -power * B * rate[c * hc + h], F32)) for h in range(hc)]
        return jnp.concatenate(rows, axis=0)

    def phase_kv(c):
        kk = rest(0, c, acc[0, c])
        vv = rest(1, c, acc[1, c])
        states = []
        for hh in range(hc):
            h = c * hc + hh
            cols = slice(hh * HEAD, (hh + 1) * HEAD)
            kr = rotated(kk[:, cols])
            tokk[h:h + 1, :] = kr[B:B + 1]
            krb = kr[:B].astype(BF)
            kbuf[h] = krb
            v = vv[:, cols]
            tokv[h:h + 1, :] = v[B:B + 1]
            vb = (v[:B] * jnp.exp(steps * rate[h])).astype(BF)
            vbuf[h] = vb
            st = lax.dot_general(krb, vb, (((0,), (0,)), ((), ())), preferred_element_type=F32)
            states.append(st * jnp.exp(jnp.full((HEAD, HEAD), -B * rate[h], F32)))
        for i in range(G):
            for zz in range(Z):
                lo = (zz * G + i) * R
                send1[c, i, zz] = jnp.concatenate([s[lo:lo + R] for s in states], axis=0).astype(BF)
        recv1[c, j] = send1[c, j]
        for d in range(1, G):
            i = lax.rem(j + d, G)
            cp = pltpu.make_async_remote_copy(
                src_ref=send1.at[c, i], dst_ref=recv1.at[c, j], send_sem=s1s.at[c, d],
                recv_sem=s1r.at[c, d], device_id={"sp": z * G + i}, device_id_type=MESH)
            cp.start()
            sends.append(cp)

    def full2(c, s, t):
        return pltpu.make_async_remote_copy(
            src_ref=recv2.at[c, s], dst_ref=recv2.at[c, s], send_sem=s2s.at[c, t],
            recv_sem=s2r.at[c, s], device_id={"sp": t * G + j}, device_id_type=MESH)

    def part2(c, s, t):
        return pltpu.make_async_remote_copy(
            src_ref=recv2.at[c, s, t], dst_ref=recv2.at[c, s, t], send_sem=s2s.at[c, t],
            recv_sem=s2r.at[c, s], device_id={"sp": t * G + j}, device_id_type=MESH)

    def phase_plane(c):
        for d in range(1, G):
            i = lax.rem(j + G - d, G)
            pltpu.make_async_remote_copy(
                src_ref=send1.at[c, i], dst_ref=recv1.at[c, i], send_sem=s1s.at[c, d],
                recv_sem=s1r.at[c, d], device_id={"sp": z * G + i}, device_id_type=MESH).wait_recv()
        gb = block_decay(c, 1)[None]
        run = jnp.zeros((Z, hc * R, HEAD), F32)
        for i in range(G):
            pre[c, i] = run
            run = run * gb + recv1[c, i].astype(F32)
        recv2[c, z] = run.astype(BF)
        for t in range(Z):
            @pl.when(t > z)
            def _():
                full2(c, z, t).start()

            @pl.when(t < z)
            def _():
                part2(c, z, t).start()

    def phase_chain(c):
        gz = block_decay(c, G)
        pacc[...] = jnp.zeros((Z, hc * R, HEAD), F32)
        for s in range(Z):
            @pl.when(s < z)
            def _():
                full2(c, s, z).wait_recv()
                pacc[...] = pacc[...] * gz[None] + recv2[c, s].astype(F32)
        run = pacc[...]
        gb = block_decay(c, 1)[None]
        for i in range(G):
            send3[c, i] = (run + pre[c, i]).astype(BF)
            run = run * gb
        recv3[c, j] = send3[c, j]
        for d in range(1, G):
            i = lax.rem(j + d, G)
            cp = pltpu.make_async_remote_copy(
                src_ref=send3.at[c, i], dst_ref=recv3.at[c, j], send_sem=s3s.at[c, d],
                recv_sem=s3r.at[c, d], device_id={"sp": z * G + i}, device_id_type=MESH)
            cp.start()
            sends.append(cp)

    def phase_final(c):
        gz = block_decay(c, G)
        run = jnp.zeros((hc * R, HEAD), F32)
        for s in range(Z):
            @pl.when(s > z)
            def _():
                part2(c, s, z).wait_recv()
            run = run * gz + recv2[c, s, z].astype(F32)
        fin[c * hc * R:(c + 1) * hc * R, :] = run
        for hh in range(hc):
            cache[c * hc + hh] = run[hh * R:(hh + 1) * R].astype(BF)

    half = B // 2
    causal = (lax.broadcasted_iota(jnp.int32, (half, half), 0)
              >= lax.broadcasted_iota(jnp.int32, (half, half), 1))

    def phase_q(c):
        wcopy(2, c, 0).wait()
        qq = rest(2, c, dot(xbuf[me], wbuf[2, c, 0]))
        for hh in range(hc):
            h = c * hc + hh
            qr = rotated(qq[:, hh * HEAD:(hh + 1) * HEAD])
            tokq[h:h + 1, :] = qr[B:B + 1]
            qb = qr[:B].astype(BF)
            qbuf[h] = qb
            for t in range(2):
                rows = qb[t * half:(t + 1) * half]
                out = None
                for s in range(t + 1):
                    ks = kbuf[h, s * half:(s + 1) * half, :]
                    sc = lax.dot_general(rows, ks, (((1,), (1,)), ((), ())), preferred_element_type=F32)
                    if s == t:
                        sc = jnp.where(causal, sc, 0.0)
                    part = dot(sc.astype(BF), vbuf[h, s * half:(s + 1) * half, :])
                    out = part if out is None else out + part
                intra[h, t * half:(t + 1) * half, :] = out

    def phase_tail(c):
        for d in range(1, G):
            i = lax.rem(j + G - d, G)
            pltpu.make_async_remote_copy(
                src_ref=send3.at[c, i], dst_ref=recv3.at[c, i], send_sem=s3s.at[c, d],
                recv_sem=s3r.at[c, d], device_id={"sp": z * G + i}, device_id_type=MESH).wait_recv()
        pieces = [[recv3[c, i, zz].astype(F32) for i in range(G)] for zz in range(Z)]
        for hh in range(hc):
            h = c * hc + hh
            inc = jnp.concatenate(
                [pieces[zz][i][hh * R:(hh + 1) * R] for zz in range(Z) for i in range(G)], axis=0)
            o = intra[h] + dot(qbuf[h], inc.astype(BF))
            o = o * (jnp.exp(steps * -rate[h]) * HEAD ** -0.5)
            res = head_norm(o, gain[:, h * HEAD:(h + 1) * HEAD])
            obuf[c, :, hh * HEAD:(hh + 1) * HEAD] = res.astype(BF)
        pltpu.make_async_copy(obuf.at[c], mixed.at[:, pl.ds(c * W, W)], o_sem.at[c]).start()

    def read_send():
        tq = tokq[...].astype(BF).astype(F32)
        n = H * R
        pick = (lax.broadcasted_iota(jnp.int32, (HEAD, n), 0)
                == rank * R + lax.broadcasted_iota(jnp.int32, (HEAD, n), 1) % R)
        sel = dot(tq, pick.astype(F32))
        own = (lax.broadcasted_iota(jnp.int32, (H, n), 0)
               == lax.broadcasted_iota(jnp.int32, (H, n), 1) // R)
        sel = jnp.where(own, sel, 0.0)
        rdbuf[rank] = jnp.dot(sel, fin[...], preferred_element_type=F32, precision=lax.Precision.HIGHEST)
        for d in range(1, M):
            peer = lax.rem(rank + d, M)
            cp = pltpu.make_async_remote_copy(
                src_ref=rdbuf.at[rank], dst_ref=rdbuf.at[rank], send_sem=rds.at[d],
                recv_sem=rdr.at[d], device_id={"sp": peer}, device_id_type=MESH)
            cp.start()
            sends.append(cp)

    def read_finish():
        for d in range(1, M):
            src = lax.rem(rank + M - d, M)
            pltpu.make_async_remote_copy(
                src_ref=rdbuf.at[src], dst_ref=rdbuf.at[src], send_sem=rds.at[d],
                recv_sem=rdr.at[d], device_id={"sp": src}, device_id_type=MESH).wait_recv()
        total = jnp.sum(rdbuf[...], axis=0)
        scale = HEAD ** -0.5
        tq = tokq[...].astype(BF).astype(F32)
        tk = tokk[...].astype(BF).astype(F32)
        score = jnp.sum(tq * tk, axis=-1, keepdims=True) * scale
        base_part = score * tokv[...].astype(BF).astype(F32)
        for h in range(H):
            g = jnp.exp(jnp.full((1, HEAD), -rate[h], F32)) * scale
            o = g * total[h:h + 1] + base_part[h:h + 1]
            read_out[:, h * HEAD:(h + 1) * HEAD] = head_norm(o, gain[:, h * HEAD:(h + 1) * HEAD]).astype(BF)

    work = [functools.partial(phase_kv, c) for c in range(NC)]
    work += [functools.partial(phase_q, c) for c in range(NC)]
    plane_at, chain_at = 2, 5
    planes = 0
    chains = 0
    for n, step in enumerate(work):
        step()
        if n >= plane_at and planes < NC and planes <= n:
            phase_plane(planes)
            planes += 1
        if n >= chain_at and chains < planes:
            phase_chain(chains)
            chains += 1
    while planes < NC:
        phase_plane(planes)
        planes += 1
    while chains < NC:
        phase_chain(chains)
        chains += 1
    for c in range(NC):
        phase_final(c)
    read_send()
    for c in range(NC):
        phase_tail(c)
    read_finish()
    for cp in sends:
        cp.wait_send()
    for c in range(NC):
        for t in range(Z):
            @pl.when(t > z)
            def _():
                full2(c, z, t).wait_send()

            @pl.when(t < z)
            def _():
                part2(c, z, t).wait_send()
        pltpu.make_async_copy(obuf.at[c], mixed.at[:, pl.ds(c * W, W)], o_sem.at[c]).wait()


def per_device(prompt, new_token, w_query, w_key, w_value, decay_rate, norm_gain):
    _, B, F = prompt.shape
    D = w_query.shape[0]
    H = w_query.shape[1] // HEAD
    M = lax.axis_size("sp")
    T = lax.axis_size("tp")
    G = split(M)
    Z = M // G
    R = HEAD // M
    hc = 2 if H % 2 == 0 else 1
    NC = H // hc
    W = hc * HEAD
    inverse = rope_base ** (-np.arange(0, HEAD, 2, dtype=np.float64) / HEAD)
    sign = np.concatenate([-np.ones(HEAD // 2), np.ones(HEAD // 2)])

    def pair(positions):
        angles = np.concatenate([positions[:, None] * inverse[None]] * 2, axis=1)
        return np.cos(angles), np.sin(angles) * sign[None]

    tab = np.stack(pair(np.arange(B, dtype=np.float64))).astype(np.float32)
    base = np.stack(pair(np.arange(M + 1, dtype=np.float64) * B), axis=1).astype(np.float32)
    any_ = pl.BlockSpec(memory_space=pltpu.HBM)
    vm = pl.BlockSpec(memory_space=pltpu.VMEM)
    sm = pl.BlockSpec(memory_space=pltpu.SMEM)
    V = pltpu.VMEM
    DMA = pltpu.SemaphoreType.DMA
    cfg = (M, G, Z, T, B, F, H, hc, R)
    mixed, cache, new_read = pl.pallas_call(
        functools.partial(kernel, cfg),
        out_shape=(
            jax.ShapeDtypeStruct((B, H * HEAD), BF),
            jax.ShapeDtypeStruct((H, R, HEAD), BF),
            jax.ShapeDtypeStruct((1, H * HEAD), BF),
        ),
        in_specs=[any_, any_, any_, any_, any_, sm, vm, any_, vm],
        out_specs=(any_, vm, vm),
        scratch_shapes=[
            V((T, B + PAD, F), BF),
            V((T, 1, F), BF),
            V((3, NC, T, F, W), BF),
            V((2, NC, B + PAD, W), F32),
            V((2, B, HEAD), F32),
            V((B + PAD, HEAD), F32),
            V((B + PAD, HEAD), F32),
            V((H, B, HEAD), BF),
            V((H, B, HEAD), BF),
            V((H, B, HEAD), BF),
            V((H, B, HEAD), F32),
            V((NC, B, W), BF),
            V((NC, G, Z, hc * R, HEAD), BF),
            V((NC, G, Z, hc * R, HEAD), BF),
            V((NC, G, Z, hc * R, HEAD), F32),
            V((NC, Z, Z, hc * R, HEAD), BF),
            V((NC, G, Z, hc * R, HEAD), BF),
            V((NC, G, Z, hc * R, HEAD), BF),
            V((Z, hc * R, HEAD), F32),
            V((H * R, HEAD), F32),
            V((H, HEAD), F32),
            V((H, HEAD), F32),
            V((H, HEAD), F32),
            V((M, H, HEAD), F32),
            DMA((3, NC, T)),
            DMA((3,)),
            DMA((2, T)),
            DMA((2, T)),
            DMA((NC, G)),
            DMA((NC, G)),
            DMA((NC, Z)),
            DMA((NC, Z)),
            DMA((NC, G)),
            DMA((NC, G)),
            DMA((M,)),
            DMA((M,)),
            DMA((NC,)),
        ],
        compiler_params=pltpu.CompilerParams(
            collective_id=0, has_side_effects=True, vmem_limit_bytes=60 * 1024 * 1024),
    )(prompt.reshape(B, F), new_token, w_query, w_key, w_value, decay_rate,
      norm_gain.reshape(1, H * HEAD), jnp.asarray(tab), jnp.asarray(base))
    return (mixed[None], cache[None], new_read)


def solution(mesh):
    in_specs = (
        P(None, "sp", "tp"),
        P(None, "tp"),
        P(None, "tp"),
        P(None, "tp"),
        P(None, "tp"),
        P("tp"),
        P("tp"),
    )
    out_specs = (P(None, "sp", "tp"), P(None, "tp", "sp", None), P(None, "tp"))
    return jax.shard_map(
        per_device, mesh=mesh, in_specs=in_specs, out_specs=out_specs, check_vma=False
    )
```

profile of v0, /device:TPU:0, one launch (start us, length us, event | category | flops | bytes accessed | tf_op | source)
XLA Modules:
  0.0 44.8 jit_solution(12046079273751028169)
XLA Ops:
  0.6 39.3 %shard_map.112 = (bf16[512,1024]{1,0:T(8,128)(2,1)}, bf16[8,8,128]{2,1,0:T(8,128)(2,1)}, bf16[1,1024]{1,0:T(2,128)(2,1)}) custom-call(bf16[512,1024]{1,0:T(8,128)(2,1)} %bitcast.4, bf16[1,1024]{1,0:T(2,128)(2,1)} %tok_hbm.1, bf16[2048,1024]{1,0:T(8,128)(2,1)} %wq.1, bf16[2048,1024]{1,0:T(8,128)(2,1)} %wk.1, bf16[2048,1024]{1,0:T(8,128)(2,1)} %wv.1, f32[8]{0:T(128)} %rate.1, ...), custom_call_target="tpu_custom_call" | custom-call | tf_op jit(solution)/shard_map/pallas_call | solution.py:386
  40.0 2.3 %copy.15 = bf16[1,512,1024]{2,1,0:T(8,128)(2,1)} copy(bf16[1,512,1024]{2,1,0:T(8,128)(2,1)} %bitcast.5) | data formatting | bytes 2097152
  42.2 1.3 %copy.16 = bf16[1,8,8,128]{3,2,1,0:T(8,128)(2,1)} copy(bf16[1,8,8,128]{3,2,1,0:T(8,128)(2,1)} %bitcast.6) | data formatting | bytes 32768
  43.6 1.3 %copy.17 = bf16[1,1024]{1,0:T(2,128)(2,1)} copy(bf16[1,1024]{1,0:T(2,128)(2,1)} %get-tuple-element.14) | data formatting | bytes 4096
where the time goes:
time: 45.1 us; the launch traced here: 44.8 us
  Pallas kernels  39.3 us (87%)
  local copies, waits for them, and re-layouts  4.85 us (11%)
  between operations  0.64 us (1%)
    pallas_call x1, Pallas kernels, per_device(): pl.pallas_call(functools.partial(kernel, cfg), out_shape=(jax.ShapeDtypeS...  39.3 us
    unnamed x3, local copies, waits for them, and re-layouts  4.85 us

commit v1 on v0

v1 whole, which is shorter than its diff:
```python
import functools

import jax
import jax.numpy as jnp
import numpy as np
from jax import lax
from jax.experimental import pallas as pl
from jax.experimental.pallas import tpu as pltpu
from jax.sharding import PartitionSpec as P

HEAD = 128
PAD = 16
rope_base = 10000.0
norm_floor = 1e-05
MESH = pl.DeviceIdType.MESH
BF = jnp.bfloat16
F32 = jnp.float32


def head_norm(o, gain):
    center = jnp.mean(o, axis=-1, keepdims=True)
    delta = o - center
    spread = jnp.mean(delta * delta, axis=-1, keepdims=True)
    return delta * lax.rsqrt(spread + norm_floor) * gain


def split(members):
    best = 1
    for g in range(1, members + 1):
        if members % g == 0 and g * g <= members:
            best = g
    return best


def dot(a, b):
    return jnp.dot(a, b, preferred_element_type=F32)


def kernel(cfg, x_hbm, tok_hbm, wq, wk, wv, rate_hbm, gain_hbm, tab_hbm, mixed, cache, read_out,
           rate, xbuf, wbuf, acc, tab, gain, ctab, stab, dec, kbuf, qbuf, vbuf, shi, slo, intra,
           send1, recv1, pre, tot, exc, upb, uprecv, down, downrecv, send3, recv3, tokq, tokk, tokv, rdbuf, tokbuf,
           w_sem, l_sem, tps, tpr, s1s, s1r, us, ur, ds, dr, s3s, s3r, rds, rdr, up_sem):
    M, G, Z, T, B, F, H, hc, R = cfg
    NC = H // hc
    W = hc * HEAD
    rank = lax.axis_index("sp")
    me = lax.axis_index("tp")
    z = rank // G
    j = rank % G
    weights = (wk, wv, wq)

    lx = pltpu.make_async_copy(x_hbm, xbuf.at[me, pl.ds(0, B)], l_sem.at[0])
    lr = pltpu.make_async_copy(rate_hbm, rate, l_sem.at[1])
    lt = pltpu.make_async_copy(tok_hbm, tokbuf, l_sem.at[2])
    ltab = pltpu.make_async_copy(tab_hbm, tab, l_sem.at[3])
    lg = pltpu.make_async_copy(gain_hbm, gain, l_sem.at[4])
    lx.start(priority=0)
    lr.start(priority=0)
    lt.start(priority=0)

    def wcopy(m, c, d, slot):
        p = lax.rem(me + d, T)
        return pltpu.make_async_copy(
            weights[m].at[pl.ds(pl.multiple_of(p * F, HEAD), F), pl.ds(c * W, W)],
            wbuf.at[m, c, d], w_sem.at[slot])

    def taken(ref, sem):
        pltpu.make_async_copy(ref, ref, sem).wait()

    for c in range(NC):
        wcopy(0, c, 0, c).start(priority=1)
        wcopy(1, c, 0, c).start(priority=1)

    barrier = pltpu.get_barrier_semaphore()
    for d in range(1, T):
        pl.semaphore_signal(barrier, inc=1, device_id={"tp": lax.rem(me + d, T)}, device_id_type=MESH)
    for d in range(1, G):
        pl.semaphore_signal(
            barrier, inc=1, device_id={"sp": z * G + lax.rem(j + d, G)}, device_id_type=MESH)
    for t in range(G, M):
        @pl.when(t // G > z)
        def _():
            pl.semaphore_signal(barrier, inc=1, device_id={"sp": t}, device_id_type=MESH)

    ltab.start(priority=1)
    for c in range(NC):
        for d in range(1, T):
            wcopy(0, c, d, NC).start(priority=1)
            wcopy(1, c, d, NC).start(priority=1)
    lg.start(priority=1)
    for c in range(NC):
        for d in range(T):
            wcopy(2, c, d, NC + 1).start(priority=1)

    lr.wait()
    ramp = (lax.broadcasted_iota(jnp.int32, (8, HEAD), 0) + 1).astype(F32)
    grow = [jnp.exp(ramp * rate[h]) for h in range(H)]
    leap = [jnp.exp(jnp.full((8, HEAD), 8.0 * rate[h], F32)) for h in range(H)]
    for n in range(0, B, 8):
        for h in range(H):
            dec[h, n:n + 8, :] = grow[h]
            grow[h] = grow[h] * leap[h]

    with jax.named_scope('w_x'):
        lx.wait()
    lt.wait()
    xbuf[me, B:B + PAD, :] = jnp.broadcast_to(tokbuf[...].astype(F32), (PAD, F)).astype(BF)

    def own_part(cs):
        for c in cs:
            taken(wbuf.at[pl.ds(0, 2), c, 0], w_sem.at[c])
        for c in cs:
            for m in range(2):
                acc[m, c] = dot(xbuf[me], wbuf[m, c, 0])

    with jax.named_scope('own0'):
        own_part([0])
    with jax.named_scope('w_bar'):
        pl.semaphore_wait(barrier, T - 1 + G - 1 + z * G)
    sends = []

    def xcopy(d, slot):
        return pltpu.make_async_remote_copy(
            src_ref=xbuf.at[slot], dst_ref=xbuf.at[slot], send_sem=tps.at[d - 1],
            recv_sem=tpr.at[d - 1], device_id={"tp": lax.rem(me + d, T)}, device_id_type=MESH)

    for d in range(1, T):
        cp = xcopy(d, me)
        cp.start()
        sends.append(cp)
    for t in range(M - G):
        @pl.when(t // G < z)
        def _():
            pl.semaphore_signal(up_sem, inc=1, device_id={"sp": t}, device_id_type=MESH)

    for cs in ([c] for c in range(1, NC)):
        with jax.named_scope(f'own{cs[0]}'):
            own_part(cs)

    ltab.wait()
    top = 2 * B
    spot = pl.multiple_of(top + rank * 16, 8)
    cb = tab[pl.ds(spot, 8), :][0:1]
    sb = tab[pl.ds(spot + 8, 8), :][0:1]
    ctab[0:B, :] = cb * tab[0:B, :] - sb * tab[B:top, :]
    stab[0:B, :] = sb * tab[0:B, :] + cb * tab[B:top, :]
    last = top + M * 16
    ctab[B:B + PAD, :] = jnp.broadcast_to(tab[last:last + 1, :], (PAD, HEAD))
    stab[B:B + PAD, :] = jnp.broadcast_to(tab[last + 8:last + 9, :], (PAD, HEAD))
    with jax.named_scope('w_wr'):
        if T > 1:
            taken(wbuf.at[pl.ds(0, 2), :, pl.ds(1, T - 1)], w_sem.at[NC])
    with jax.named_scope('w_tpx'):
        for d in range(1, T):
            xcopy(d, lax.rem(me + T - d, T)).wait_recv()

    def rotated(u):
        return u * ctab[...] + pltpu.roll(u, HEAD // 2, 1) * stab[...]

    def block_decay(c, power):
        rows = [jnp.exp(jnp.full((R, HEAD), -power * B * rate[c * hc + h], F32)) for h in range(hc)]
        return jnp.concatenate(rows, axis=0)

    def kv_dots(c):
        for m in range(2):
            total = acc[m, c]
            for d in range(1, T):
                total = total + dot(xbuf[lax.rem(me + d, T)], wbuf[m, c, d])
            acc[m, c] = total

    def kv_finish(c):
        states = []
        for hh in range(hc):
            h = c * hc + hh
            cols = slice(hh * HEAD, (hh + 1) * HEAD)
            kr = rotated(acc[0, c, :, cols])
            tokk[h:h + 1, :] = kr[B:B + 1]
            krb = kr[:B].astype(BF)
            kbuf[h] = krb
            v = acc[1, c, :, cols]
            tokv[h:h + 1, :] = v[B:B + 1]
            vb = (v[:B] * dec[h]).astype(BF)
            vbuf[h] = vb
            st = lax.dot_general(krb, vb, (((0,), (0,)), ((), ())), preferred_element_type=F32)
            st = st * jnp.exp(jnp.full((HEAD, HEAD), -B * rate[h], F32))
            hi = st.astype(BF)
            shi[h] = hi
            slo[h] = (st - hi.astype(F32)).astype(BF)
            states.append(st)
        for i in range(G):
            for zz in range(Z):
                lo = (zz * G + i) * R
                send1[c, i, zz] = jnp.concatenate([s[lo:lo + R] for s in states], axis=0).astype(BF)
        recv1[c, j] = send1[c, j]

    def kv_send(c):
        for d in range(1, G):
            i = lax.rem(j + d, G)
            cp = pltpu.make_async_remote_copy(
                src_ref=send1.at[c, i], dst_ref=recv1.at[c, j], send_sem=s1s.at[0],
                recv_sem=s1r.at[c], device_id={"sp": z * G + i}, device_id_type=MESH)
            cp.start()

    def plane_wait(c):
        taken(recv1.at[c, pl.ds(0, G - 1)], s1r.at[c])

    def faded(c, p):
        rows = [jnp.exp(jnp.full((R, HEAD), -G * B * rate[c * hc + h], F32) * p) for h in range(hc)]
        return jnp.concatenate(rows, axis=0)[None]

    levels = (Z - 1).bit_length()

    def up_send(c, level):
        if level >= levels:
            return

        @pl.when(z % (2 << level) == (1 << level) - 1)
        def _():
            upb[c] = (tot[c] + exc[c] * faded(c, 1.0)).astype(BF)
            for k in range(1, (1 << level) + 1):
                @pl.when(z + k < Z)
                def _():
                    pltpu.make_async_remote_copy(
                        src_ref=upb.at[c], dst_ref=uprecv.at[c, level], send_sem=us.at[0],
                        recv_sem=ur.at[c, level], device_id={"sp": (z + k) * G + j},
                        device_id_type=MESH).start()

    def plane(c):
        gb = block_decay(c, 1)[None]
        run = jnp.zeros((Z, hc * R, HEAD), F32)
        for i in range(G):
            pre[c, i] = run
            run = run * gb + recv1[c, i].astype(F32)
        tot[c] = run
        exc[c] = jnp.zeros((Z, hc * R, HEAD), F32)
        down[c] = run.astype(BF)
        for t in range(Z):
            @pl.when(t < z)
            def _():
                pltpu.make_async_remote_copy(
                    src_ref=down.at[c, t], dst_ref=downrecv.at[c, z], send_sem=ds.at[0],
                    recv_sem=dr.at[0], device_id={"sp": t * G + j}, device_id_type=MESH).start()
        up_send(c, 0)

    def climb(c, level):
        @pl.when((z // (1 << level)) % 2 == 1)
        def _():
            taken(uprecv.at[c, level], ur.at[c, level])
            p = (z % (1 << level)).astype(F32)
            exc[c] = exc[c] + uprecv[c, level].astype(F32) * faded(c, p)
        up_send(c, level + 1)

    def give_back(c):
        run = exc[c]
        gb = block_decay(c, 1)[None]
        for i in range(G):
            send3[c, i] = (run + pre[c, i]).astype(BF)
            run = run * gb
        recv3[c, j] = send3[c, j]
        for d in range(1, G):
            i = lax.rem(j + d, G)
            cp = pltpu.make_async_remote_copy(
                src_ref=send3.at[c, i], dst_ref=recv3.at[c, j], send_sem=s3s.at[0],
                recv_sem=s3r.at[c], device_id={"sp": z * G + i}, device_id_type=MESH)
            cp.start()

    def final():
        for k in range(1, Z):
            @pl.when(Z - 1 - z == k)
            def _():
                taken(downrecv.at[:, pl.ds(0, k)], dr.at[0])
        for c in range(NC):
            gz = faded(c, 1.0)[0]
            run = tot[c, z] + exc[c, z] * gz
            for s in range(1, Z):
                run = jnp.where(s > z, run * gz + downrecv[c, s].astype(F32), run)
            for hh in range(hc):
                cache[c * hc + hh] = run[hh * R:(hh + 1) * R].astype(BF)

    def q_project(cs):
        totals = []
        for c in cs:
            total = dot(xbuf[me], wbuf[2, c, 0])
            for d in range(1, T):
                total = total + dot(xbuf[lax.rem(me + d, T)], wbuf[2, c, d])
            totals.append(total)
        for c, total in zip(cs, totals):
            for hh in range(hc):
                h = c * hc + hh
                qr = rotated(total[:, hh * HEAD:(hh + 1) * HEAD])
                tokq[h:h + 1, :] = qr[B:B + 1]
                qbuf[h] = qr[:B].astype(BF)

    half = B // 2
    causal = (lax.broadcasted_iota(jnp.int32, (half, half), 0)
              >= lax.broadcasted_iota(jnp.int32, (half, half), 1))

    def attend(c):
        for hh in range(hc):
            h = c * hc + hh
            for t in range(2):
                rows = qbuf[h, t * half:(t + 1) * half, :]
                out = None
                for s in range(t + 1):
                    ks = kbuf[h, s * half:(s + 1) * half, :]
                    sc = lax.dot_general(rows, ks, (((1,), (1,)), ((), ())), preferred_element_type=F32)
                    if s == t:
                        sc = jnp.where(causal, sc, 0.0)
                    part = dot(sc.astype(BF), vbuf[h, s * half:(s + 1) * half, :])
                    out = part if out is None else out + part
                intra[h, t * half:(t + 1) * half, :] = out

    def tail_wait(c):
        taken(recv3.at[c, pl.ds(0, G - 1)], s3r.at[c])

    def tail(c):
        pieces = [[recv3[c, i, zz].astype(F32) for i in range(G)] for zz in range(Z)]
        for hh in range(hc):
            h = c * hc + hh
            inc = jnp.concatenate(
                [pieces[zz][i][hh * R:(hh + 1) * R] for zz in range(Z) for i in range(G)], axis=0)
            o = intra[h] + dot(qbuf[h], inc.astype(BF))
            delta = o - jnp.mean(o, axis=-1, keepdims=True)
            spread = jnp.mean(delta * delta, axis=-1, keepdims=True)
            up = dec[h]
            res = delta * lax.rsqrt(spread + (norm_floor * HEAD) * (up * up)) * gain[:, h * HEAD:(h + 1) * HEAD]
            mixed[:, h * HEAD:(h + 1) * HEAD] = res.astype(BF)

    def read_send():
        tq = jnp.concatenate([tokq[...], tokq[...]], axis=0).astype(BF)
        later = (M - 1 - rank).astype(F32)
        for h in range(H):
            got = dot(tq, shi[h]) + dot(tq, slo[h])
            fade = jnp.exp(jnp.full((1, HEAD), -B * rate[h], F32) * later)
            rdbuf[rank, h:h + 1, :] = got[h:h + 1] * fade
        for d in range(1, M):
            peer = lax.rem(rank + d, M)
            cp = pltpu.make_async_remote_copy(
                src_ref=rdbuf.at[rank], dst_ref=rdbuf.at[rank], send_sem=rds.at[0],
                recv_sem=rdr.at[0], device_id={"sp": peer}, device_id_type=MESH)
            cp.start()

    def read_finish():
        taken(rdbuf.at[pl.ds(0, M - 1)], rdr.at[0])
        total = jnp.sum(rdbuf[...], axis=0)
        scale = HEAD ** -0.5
        tq = tokq[...].astype(BF).astype(F32)
        tk = tokk[...].astype(BF).astype(F32)
        score = jnp.sum(tq * tk, axis=-1, keepdims=True) * scale
        base_part = score * tokv[...].astype(BF).astype(F32)
        for h in range(H):
            g = jnp.exp(jnp.full((1, HEAD), -rate[h], F32)) * scale
            o = g * total[h:h + 1] + base_part[h:h + 1]
            read_out[:, h * HEAD:(h + 1) * HEAD] = head_norm(o, gain[:, h * HEAD:(h + 1) * HEAD]).astype(BF)

    for c in range(NC):
        with jax.named_scope(f"kv{c}"):
            kv_dots(c)
            if c > 0:
                kv_finish(c - 1)
                kv_send(c - 1)
    with jax.named_scope("kvlast"):
        kv_finish(NC - 1)
        kv_send(NC - 1)
    with jax.named_scope("w_wq"):
        taken(wbuf.at[2], w_sem.at[NC + 1])
    groups = [range(c, min(c + 2, NC)) for c in range(0, NC, 2)]
    for n, cs in enumerate(groups):
        with jax.named_scope(f"q{n}"):
            q_project(cs)
    with jax.named_scope("w_up"):
        @pl.when(z < Z - 1)
        def _():
            pl.semaphore_wait(up_sem, (Z - 1 - z) * G)
    lg.wait()
    with jax.named_scope("rsend"):
        read_send()
    for c in range(NC):
        with jax.named_scope(f"w_plane{c}"):
            plane_wait(c)
        with jax.named_scope(f"plane{c}"):
            plane(c)
    todo = [[] for _ in range(NC)]
    for level in range(levels):
        for c in range(NC):
            todo[min(level, NC - 1)].append((c, level))
    for c in range(NC):
        with jax.named_scope(f"att{c}"):
            attend(c)
        for cc, level in todo[c]:
            with jax.named_scope(f"climb{cc}_{level}"):
                climb(cc, level)
                if level == levels - 1:
                    give_back(cc)
    with jax.named_scope("final"):
        final()
    for c in range(NC):
        with jax.named_scope(f"w_tail{c}"):
            tail_wait(c)
        with jax.named_scope(f"tail{c}"):
            tail(c)
    with jax.named_scope("rfin"):
        read_finish()
    with jax.named_scope("w_sends"):
        for cp in sends:
            cp.wait_send()
        taken(send1.at[:, pl.ds(0, G - 1)], s1s.at[0])
        taken(send3.at[:, pl.ds(0, G - 1)], s3s.at[0])
        taken(rdbuf.at[pl.ds(0, M - 1)], rds.at[0])
        for k in range(1, Z):
            @pl.when(z == k)
            def _():
                taken(down.at[:, pl.ds(0, k)], ds.at[0])
        for k in range(Z - 1):
            level = ((k + 1) & -(k + 1)).bit_length() - 1
            count = min(1 << level, Z - 1 - k)

            @pl.when(z == k)
            def _():
                taken(uprecv.at[:, pl.ds(0, 1)] if count == 1 else recv1.at[:, pl.ds(0, count)], us.at[0])


def flush(*refs):
    n = len(refs) // 2
    sems = refs[-1]
    copies = [pltpu.make_async_copy(refs[i], refs[n + i], sems.at[i]) for i in range(n)]
    for cp in copies:
        cp.start()
    for cp in copies:
        cp.wait()


def per_device(prompt, new_token, w_query, w_key, w_value, decay_rate, norm_gain):
    _, B, F = prompt.shape
    H = w_query.shape[1] // HEAD
    M = lax.axis_size("sp")
    T = lax.axis_size("tp")
    G = split(M)
    Z = M // G
    R = HEAD // M
    hc = 2 if H % 2 == 0 else 1
    NC = H // hc
    W = hc * HEAD
    inverse = rope_base ** (-np.arange(0, HEAD, 2, dtype=np.float64) / HEAD)
    sign = np.concatenate([-np.ones(HEAD // 2), np.ones(HEAD // 2)])

    def pair(positions):
        angles = np.concatenate([positions[:, None] * inverse[None]] * 2, axis=1)
        return np.cos(angles), np.sin(angles) * sign[None]

    tab = np.stack(pair(np.arange(B, dtype=np.float64))).astype(np.float32)
    base = np.stack(pair(np.arange(M + 1, dtype=np.float64) * B), axis=1).astype(np.float32)
    tab = np.concatenate([tab.reshape(2 * B, HEAD), np.repeat(base.reshape(2 * (M + 1), HEAD), 8, axis=0)])
    levels = (Z - 1).bit_length()
    any_ = pl.BlockSpec(memory_space=pltpu.HBM)
    vm = pl.BlockSpec(memory_space=pltpu.VMEM)
    V = pltpu.VMEM
    DMA = pltpu.SemaphoreType.DMA
    cfg = (M, G, Z, T, B, F, H, hc, R)
    shapes = ((B, H * HEAD), (H, R, HEAD), (1, H * HEAD))
    held = pl.pallas_call(
        functools.partial(kernel, cfg),
        out_shape=tuple(V(shape, BF) for shape in shapes),
        in_specs=[any_] * 8,
        out_specs=(vm, vm, vm),
        scratch_shapes=[
            pltpu.SMEM((H,), F32),
            V((T, B + PAD, F), BF),
            V((3, NC, T, F, W), BF),
            V((2, NC, B + PAD, W), F32),
            V(tab.shape, F32),
            V((1, H * HEAD), F32),
            V((B + PAD, HEAD), F32),
            V((B + PAD, HEAD), F32),
            V((H, B, HEAD), F32),
            V((H, B, HEAD), BF),
            V((H, B, HEAD), BF),
            V((H, B, HEAD), BF),
            V((H, HEAD, HEAD), BF),
            V((H, HEAD, HEAD), BF),
            V((H, B, HEAD), F32),
            V((NC, G, Z, hc * R, HEAD), BF),
            V((NC, G, Z, hc * R, HEAD), BF),
            V((NC, G, Z, hc * R, HEAD), F32),
            V((NC, Z, hc * R, HEAD), F32),
            V((NC, Z, hc * R, HEAD), F32),
            V((NC, Z, hc * R, HEAD), BF),
            V((NC, max(levels, 1), Z, hc * R, HEAD), BF),
            V((NC, Z, hc * R, HEAD), BF),
            V((NC, Z, hc * R, HEAD), BF),
            V((NC, G, Z, hc * R, HEAD), BF),
            V((NC, G, Z, hc * R, HEAD), BF),
            V((H, HEAD), F32),
            V((H, HEAD), F32),
            V((H, HEAD), F32),
            V((M, H, HEAD), F32),
            V((1, F), BF),
            DMA((NC + 2,)),
            DMA((5,)),
            DMA((max(T - 1, 1),)),
            DMA((max(T - 1, 1),)),
            DMA((1,)),
            DMA((NC,)),
            DMA((1,)),
            DMA((NC, max(levels, 1))),
            DMA((1,)),
            DMA((1,)),
            DMA((1,)),
            DMA((NC,)),
            DMA((1,)),
            DMA((1,)),
            pltpu.SemaphoreType.REGULAR,
        ],
        compiler_params=pltpu.CompilerParams(
            collective_id=0, has_side_effects=True, vmem_limit_bytes=60 * 1024 * 1024),
    )(prompt.reshape(B, F), new_token, w_query, w_key, w_value, decay_rate,
      norm_gain.reshape(1, H * HEAD), jnp.asarray(tab, F32))
    mixed, cache, new_read = pl.pallas_call(
        flush,
        out_shape=tuple(jax.ShapeDtypeStruct(shape, BF) for shape in shapes),
        in_specs=[vm] * len(shapes),
        out_specs=(any_,) * len(shapes),
        scratch_shapes=[DMA((len(shapes),))],
    )(*(pltpu.with_memory_space_constraint(a, V) for a in held))
    return (mixed[None], cache[None], new_read)


def solution(mesh):
    in_specs = (
        P(None, "sp", "tp"),
        P(None, "tp"),
        P(None, "tp"),
        P(None, "tp"),
        P(None, "tp"),
        P("tp"),
        P("tp"),
    )
    out_specs = (P(None, "sp", "tp"), P(None, "tp", "sp", None), P(None, "tp"))
    return jax.shard_map(
        per_device, mesh=mesh, in_specs=in_specs, out_specs=out_specs, check_vma=False
    )
```

time: 45.1 us -> 25.5 us (0.57)
  the two profiles are of different devices: /device:TPU:0 before, /device:TPU:16 now
where the time goes in v1:
time: 25.5 us; the launch traced here: 25.3 us
  Pallas kernels  24.7 us (97%)
  between operations  0.64 us (3%)
    pallas_call x1, Pallas kernels, per_device(): pl.pallas_call(functools.partial(kernel, cfg), out_shape=tuple((V(shape,...  23.7 us
    pallas_call x1, Pallas kernels, per_device(): pl.pallas_call(flush, out_shape=tuple((jax.ShapeDtypeStruct(shape, BF) fo...  1 us

profile of v1, /device:TPU:16, one launch (start us, length us, event | category | flops | bytes accessed | tf_op | source)
XLA Modules:
  0.0 25.3 jit_solution(8836143280001456702)
XLA Ops:
  0.6 23.7 %shard_map.103 = (bf16[512,1024]{1,0:T(8,128)(2,1)S(1)}, bf16[8,8,128]{2,1,0:T(8,128)(2,1)S(1)}, bf16[1,1024]{1,0:T(2,128)(2,1)S(1)}) custom-call(bf16[512,1024]{1,0:T(8,128)(2,1)} %bitcast.4, bf16[1,1024]{1,0:T(2,128)(2,1)} %tok_hbm.1, bf16[2048,1024]{1,0:T(8,128)(2,1)} %wq.1, bf16[2048,1024]{1,0:T(8,128)(2,1)} %wk.1, bf16[2048,1024]{1,0:T(8,128)(2,1)} %wv.1, ...), custom_call_target="tpu_custom_call" | custom-call | tf_op jit(solution)/shard_map/pallas_call | solution.py:461
  24.3 1.0 %shard_map.104 = (bf16[512,1024]{1,0:T(8,128)(2,1)}, bf16[8,8,128]{2,1,0:T(8,128)(2,1)}, bf16[1,1024]{1,0:T(2,128)(2,1)}) custom-call(bf16[512,1024]{1,0:T(8,128)(2,1)S(1)} %get-tuple-element.9.refs_0_, bf16[8,8,128]{2,1,0:T(8,128)(2,1)S(1)} %get-tuple-element.10.refs_1_, bf16[1,1024]{1,0:T(2,128)(2,1)S(1)} %get-tuple-element.11.refs_2_), custom_call_target="tpu_custom_call" | custom-call | tf_op jit(solution)/shard_map/pallas_call | solution.py:518

commit v2 on v1

--- a/solution.py
+++ b/solution.py
@@ -37,8 +37,8 @@
 
 
 def kernel(cfg, x_hbm, tok_hbm, wq, wk, wv, rate_hbm, gain_hbm, tab_hbm, mixed, cache, read_out,
-           rate, xbuf, wbuf, acc, tab, gain, ctab, stab, dec, kbuf, qbuf, vbuf, shi, slo, intra,
-           send1, recv1, pre, tot, exc, upb, uprecv, down, downrecv, send3, recv3, tokq, tokk, tokv, rdbuf, tokbuf,
+           rate, xbuf, wbuf, acc, tab, gain, ctab, stab, dec, floor, kbuf, qbuf, vbuf, early, shi, slo, intra,
+           send1, recv1, pre, tot, exc, upb, uprecv, down, downrecv, send3, recv3, tokq, tokk, tokv, rd1, rd2, rd3, tokbuf,
            w_sem, l_sem, tps, tpr, s1s, s1r, us, ur, ds, dr, s3s, s3r, rds, rdr, up_sem):
     M, G, Z, T, B, F, H, hc, R = cfg
     NC = H // hc
@@ -70,6 +70,7 @@
     for c in range(NC):
         wcopy(0, c, 0, c).start(priority=1)
         wcopy(1, c, 0, c).start(priority=1)
+    ltab.start(priority=1)
 
     barrier = pltpu.get_barrier_semaphore()
     for d in range(1, T):
@@ -77,20 +78,17 @@
     for d in range(1, G):
         pl.semaphore_signal(
             barrier, inc=1, device_id={"sp": z * G + lax.rem(j + d, G)}, device_id_type=MESH)
-    for t in range(G, M):
-        @pl.when(t // G > z)
+    for t in range(1, Z):
+        @pl.when(t > z)
         def _():
-            pl.semaphore_signal(barrier, inc=1, device_id={"sp": t}, device_id_type=MESH)
-
-    ltab.start(priority=1)
+            for i in range(G):
+                pl.semaphore_signal(
+                    barrier, inc=1, device_id={"sp": t * G + i}, device_id_type=MESH)
+
     for c in range(NC):
         for d in range(1, T):
             wcopy(0, c, d, NC).start(priority=1)
             wcopy(1, c, d, NC).start(priority=1)
-    lg.start(priority=1)
-    for c in range(NC):
-        for d in range(T):
-            wcopy(2, c, d, NC + 1).start(priority=1)
 
     lr.wait()
     ramp = (lax.broadcasted_iota(jnp.int32, (8, HEAD), 0) + 1).astype(F32)
@@ -99,6 +97,7 @@
     for n in range(0, B, 8):
         for h in range(H):
             dec[h, n:n + 8, :] = grow[h]
+            floor[h, n:n + 8, :] = grow[h] * grow[h] * (norm_floor * HEAD)
             grow[h] = grow[h] * leap[h]
 
     with jax.named_scope('w_x'):
@@ -128,14 +127,19 @@
         cp = xcopy(d, me)
         cp.start()
         sends.append(cp)
-    for t in range(M - G):
-        @pl.when(t // G < z)
+    lg.start(priority=1)
+    for c in range(NC):
+        for d in range(T):
+            wcopy(2, c, d, NC + 1).start(priority=1)
+    for t in range(Z - 1):
+        @pl.when(t < z)
         def _():
-            pl.semaphore_signal(up_sem, inc=1, device_id={"sp": t}, device_id_type=MESH)
-
-    for cs in ([c] for c in range(1, NC)):
-        with jax.named_scope(f'own{cs[0]}'):
-            own_part(cs)
+            pl.semaphore_signal(up_sem, inc=1, device_id={"sp": t * G + j}, device_id_type=MESH)
+
+    for cs in ([c] for c in range(1, NC // 2)):
+        own_part(cs)
+    with jax.named_scope("own_last"):
+        own_part(range(max(NC // 2, 1), NC))
 
     ltab.wait()
     top = 2 * B
@@ -161,6 +165,10 @@
         rows = [jnp.exp(jnp.full((R, HEAD), -power * B * rate[c * hc + h], F32)) for h in range(hc)]
         return jnp.concatenate(rows, axis=0)
 
+    half = B // 2
+    causal = (lax.broadcasted_iota(jnp.int32, (half, half), 0)
+              >= lax.broadcasted_iota(jnp.int32, (half, half), 1))
+
     def kv_dots(c):
         for m in range(2):
             total = acc[m, c]
@@ -179,10 +187,14 @@
             kbuf[h] = krb
             v = acc[1, c, :, cols]
             tokv[h:h + 1, :] = v[B:B + 1]
-            vb = (v[:B] * dec[h]).astype(BF)
-            vbuf[h] = vb
-            st = lax.dot_general(krb, vb, (((0,), (0,)), ((), ())), preferred_element_type=F32)
-            st = st * jnp.exp(jnp.full((HEAD, HEAD), -B * rate[h], F32))
+            vd = v[:B] * dec[h]
+            vb = vd.astype(BF)
+            vbuf[h] = (vd - jnp.mean(vd, axis=-1, keepdims=True)).astype(BF)
+            first, second = (
+                lax.dot_general(krb[lo:lo + half], vb[lo:lo + half], (((0,), (0,)), ((), ())), preferred_element_type=F32)
+                for lo in (0, half))
+            early[h] = first
+            st = (first + second) * jnp.exp(jnp.full((HEAD, HEAD), -B * rate[h], F32))
             hi = st.astype(BF)
             shi[h] = hi
             slo[h] = (st - hi.astype(F32)).astype(BF)
@@ -217,7 +229,7 @@
         @pl.when(z % (2 << level) == (1 << level) - 1)
         def _():
             upb[c] = (tot[c] + exc[c] * faded(c, 1.0)).astype(BF)
-            for k in range(1, (1 << level) + 1):
+            for k in range(1 << level, 0, -1):
                 @pl.when(z + k < Z)
                 def _():
                     pltpu.make_async_remote_copy(
@@ -242,6 +254,10 @@
                     recv_sem=dr.at[0], device_id={"sp": t * G + j}, device_id_type=MESH).start()
         up_send(c, 0)
 
+        @pl.when(z == 0)
+        def _():
+            give_back(c)
+
     def climb(c, level):
         @pl.when((z // (1 << level)) % 2 == 1)
         def _():
@@ -249,6 +265,10 @@
             p = (z % (1 << level)).astype(F32)
             exc[c] = exc[c] + uprecv[c, level].astype(F32) * faded(c, p)
         up_send(c, level + 1)
+
+        @pl.when(z // (1 << level) == 1)
+        def _():
+            give_back(c)
 
     def give_back(c):
         run = exc[c]
@@ -291,24 +311,15 @@
                 tokq[h:h + 1, :] = qr[B:B + 1]
                 qbuf[h] = qr[:B].astype(BF)
 
-    half = B // 2
-    causal = (lax.broadcasted_iota(jnp.int32, (half, half), 0)
-              >= lax.broadcasted_iota(jnp.int32, (half, half), 1))
-
     def attend(c):
         for hh in range(hc):
             h = c * hc + hh
-            for t in range(2):
-                rows = qbuf[h, t * half:(t + 1) * half, :]
-                out = None
-                for s in range(t + 1):
-                    ks = kbuf[h, s * half:(s + 1) * half, :]
-                    sc = lax.dot_general(rows, ks, (((1,), (1,)), ((), ())), preferred_element_type=F32)
-                    if s == t:
-                        sc = jnp.where(causal, sc, 0.0)
-                    part = dot(sc.astype(BF), vbuf[h, s * half:(s + 1) * half, :])
-                    out = part if out is None else out + part
-                intra[h, t * half:(t + 1) * half, :] = out
+            for lo in (0, half):
+                at = slice(lo, lo + half)
+                sc = lax.dot_general(
+                    qbuf[h, at, :], kbuf[h, at, :], (((1,), (1,)), ((), ())), preferred_element_type=F32)
+                sc = jnp.where(causal, sc, 0.0).astype(BF)
+                intra[h, at, :] = dot(sc, vbuf[h, at, :])
 
     def tail_wait(c):
         taken(recv3.at[c, pl.ds(0, G - 1)], s3r.at[c])
@@ -319,12 +330,14 @@
             h = c * hc + hh
             inc = jnp.concatenate(
                 [pieces[zz][i][hh * R:(hh + 1) * R] for zz in range(Z) for i in range(G)], axis=0)
-            o = intra[h] + dot(qbuf[h], inc.astype(BF))
-            delta = o - jnp.mean(o, axis=-1, keepdims=True)
-            spread = jnp.mean(delta * delta, axis=-1, keepdims=True)
-            up = dec[h]
-            res = delta * lax.rsqrt(spread + (norm_floor * HEAD) * (up * up)) * gain[:, h * HEAD:(h + 1) * HEAD]
-            mixed[:, h * HEAD:(h + 1) * HEAD] = res.astype(BF)
+            for lo in (0, half):
+                at = slice(lo, lo + half)
+                held = inc if lo == 0 else inc + early[h]
+                held = (held - jnp.mean(held, axis=-1, keepdims=True)).astype(BF)
+                delta = intra[h, at, :] + dot(qbuf[h, at, :], held)
+                spread = jnp.mean(delta * delta, axis=-1, keepdims=True)
+                res = delta * lax.rsqrt(spread + floor[h, at, :]) * gain[:, h * HEAD:(h + 1) * HEAD]
+                mixed[at, h * HEAD:(h + 1) * HEAD] = res.astype(BF)
 
     def read_send():
         tq = jnp.concatenate([tokq[...], tokq[...]], axis=0).astype(BF)
@@ -332,17 +345,44 @@
         for h in range(H):
             got = dot(tq, shi[h]) + dot(tq, slo[h])
             fade = jnp.exp(jnp.full((1, HEAD), -B * rate[h], F32) * later)
-            rdbuf[rank, h:h + 1, :] = got[h:h + 1] * fade
-        for d in range(1, M):
-            peer = lax.rem(rank + d, M)
-            cp = pltpu.make_async_remote_copy(
-                src_ref=rdbuf.at[rank], dst_ref=rdbuf.at[rank], send_sem=rds.at[0],
-                recv_sem=rdr.at[0], device_id={"sp": peer}, device_id_type=MESH)
-            cp.start()
+            rd1[j, h:h + 1, :] = got[h:h + 1] * fade
+        for d in range(1, G):
+            pltpu.make_async_remote_copy(
+                src_ref=rd1.at[j], dst_ref=rd1.at[j], send_sem=rds.at[0], recv_sem=rdr.at[0],
+                device_id={"sp": z * G + lax.rem(j + d, G)}, device_id_type=MESH).start()
+        for t in range(Z - 1):
+            @pl.when(t < z)
+            def _():
+                for i in range(G):
+                    pltpu.make_async_remote_copy(
+                        src_ref=rd1.at[j], dst_ref=rd3.at[rank], send_sem=rds.at[1], recv_sem=rdr.at[1],
+                        device_id={"sp": t * G + i}, device_id_type=MESH).start()
+
+    def read_relay():
+        taken(rd1.at[pl.ds(0, G - 1)], rdr.at[0])
+        rd2[z] = jnp.sum(rd1[...], axis=0)
+        for t in range(1, Z):
+            @pl.when(t > z)
+            def _():
+                pltpu.make_async_remote_copy(
+                    src_ref=rd2.at[z], dst_ref=rd2.at[z], send_sem=rds.at[2], recv_sem=rdr.at[2],
+                    device_id={"sp": t * G + j}, device_id_type=MESH).start()
 
     def read_finish():
-        taken(rdbuf.at[pl.ds(0, M - 1)], rdr.at[0])
-        total = jnp.sum(rdbuf[...], axis=0)
+        for k in range(1, Z):
+            @pl.when(Z - 1 - z == k)
+            def _():
+                taken(rd3.at[pl.ds(0, k * G)], rdr.at[1])
+
+            @pl.when(z == k)
+            def _():
+                taken(rd2.at[pl.ds(0, k)], rdr.at[2])
+        total = rd2[z]
+        for t in range(Z):
+            if t < Z - 1:
+                total = total + jnp.where(t < z, rd2[t], 0.0)
+            if t > 0:
+                total = total + jnp.where(t > z, jnp.sum(rd3[t * G:(t + 1) * G], axis=0), 0.0)
         scale = HEAD ** -0.5
         tq = tokq[...].astype(BF).astype(F32)
         tk = tokk[...].astype(BF).astype(F32)
@@ -353,7 +393,35 @@
             o = g * total[h:h + 1] + base_part[h:h + 1]
             read_out[:, h * HEAD:(h + 1) * HEAD] = head_norm(o, gain[:, h * HEAD:(h + 1) * HEAD]).astype(BF)
 
+    def before_q():
+        with jax.named_scope("w_up"):
+            @pl.when(z < Z - 1)
+            def _():
+                pl.semaphore_wait(up_sem, Z - 1 - z)
+        lg.wait()
+        with jax.named_scope("w_wq"):
+            taken(wbuf.at[2], w_sem.at[NC + 1])
+
+    def planes(cs):
+        for c in cs:
+            with jax.named_scope(f"w_plane{c}"):
+                plane_wait(c)
+            with jax.named_scope(f"plane{c}"):
+                plane(c)
+
+    def attends(cs):
+        for c in cs:
+            with jax.named_scope(f"att{c}"):
+                attend(c)
+
+    def climbs(cs, level):
+        for c in cs:
+            with jax.named_scope(f"climb{c}_{level}"):
+                climb(c, level)
+
     for c in range(NC):
+        if c == NC - 1:
+            before_q()
         with jax.named_scope(f"kv{c}"):
             kv_dots(c)
             if c > 0:
@@ -362,55 +430,74 @@
     with jax.named_scope("kvlast"):
         kv_finish(NC - 1)
         kv_send(NC - 1)
-    with jax.named_scope("w_wq"):
-        taken(wbuf.at[2], w_sem.at[NC + 1])
     groups = [range(c, min(c + 2, NC)) for c in range(0, NC, 2)]
+    ready = 0
     for n, cs in enumerate(groups):
         with jax.named_scope(f"q{n}"):
             q_project(cs)
-    with jax.named_scope("w_up"):
-        @pl.when(z < Z - 1)
-        def _():
-            pl.semaphore_wait(up_sem, (Z - 1 - z) * G)
-    lg.wait()
+        if n < len(groups) - 1:
+            for c in cs:
+                attends([c])
+                planes([ready])
+                ready += 1
+    planes(range(ready, NC))
     with jax.named_scope("rsend"):
         read_send()
-    for c in range(NC):
-        with jax.named_scope(f"w_plane{c}"):
-            plane_wait(c)
-        with jax.named_scope(f"plane{c}"):
-            plane(c)
-    todo = [[] for _ in range(NC)]
-    for level in range(levels):
-        for c in range(NC):
-            todo[min(level, NC - 1)].append((c, level))
-    for c in range(NC):
-        with jax.named_scope(f"att{c}"):
-            attend(c)
-        for cc, level in todo[c]:
-            with jax.named_scope(f"climb{cc}_{level}"):
-                climb(cc, level)
-                if level == levels - 1:
-                    give_back(cc)
-    with jax.named_scope("final"):
-        final()
-    for c in range(NC):
-        with jax.named_scope(f"w_tail{c}"):
-            tail_wait(c)
-        with jax.named_scope(f"tail{c}"):
-            tail(c)
-    with jax.named_scope("rfin"):
-        read_finish()
+    rest = list(groups[-1])
+    step = 0
+    if levels > 0:
+        climbs([0], 0)
+        step = 1
+    for c in rest:
+        attends([c])
+        if levels > 0:
+            more = NC if c == rest[-1] else min(step + 1, NC)
+            climbs(range(step, more), 0)
+            step = more
+    for level in range(1, levels):
+        climbs(range(NC), level)
+    with jax.named_scope("w_relay"):
+        read_relay()
+    middle = Z // 2
+
+    @pl.when(z >= middle)
+    def _():
+        with jax.named_scope("finala"):
+            final()
+    for n, cs in enumerate(groups):
+        with jax.named_scope(f"w_tail{cs[0]}"):
+            for c in cs:
+                tail_wait(c)
+        with jax.named_scope(f"tail{cs[0]}"):
+            for c in cs:
+                tail(c)
+        if n == 0:
+            @pl.when(z >= middle)
+            def _():
+                with jax.named_scope("w_rfina"):
+                    read_finish()
+
+    @pl.when(z < middle)
+    def _():
+        with jax.named_scope("final"):
+            final()
+        with jax.named_scope("w_rfin"):
+            read_finish()
     with jax.named_scope("w_sends"):
         for cp in sends:
             cp.wait_send()
         taken(send1.at[:, pl.ds(0, G - 1)], s1s.at[0])
         taken(send3.at[:, pl.ds(0, G - 1)], s3s.at[0])
-        taken(rdbuf.at[pl.ds(0, M - 1)], rds.at[0])
+        taken(rd1.at[pl.ds(0, G - 1)], rds.at[0])
         for k in range(1, Z):
             @pl.when(z == k)
             def _():
                 taken(down.at[:, pl.ds(0, k)], ds.at[0])
+                taken(rd3.at[pl.ds(0, k * G)], rds.at[1])
+
+            @pl.when(Z - 1 - z == k)
+            def _():
+                taken(rd2.at[pl.ds(0, k)], rds.at[2])
         for k in range(Z - 1):
             level = ((k + 1) & -(k + 1)).bit_length() - 1
             count = min(1 << level, Z - 1 - k)
@@ -473,9 +560,11 @@
             V((B + PAD, HEAD), F32),
             V((B + PAD, HEAD), F32),
             V((H, B, HEAD), F32),
+            V((H, B, HEAD), F32),
             V((H, B, HEAD), BF),
             V((H, B, HEAD), BF),
             V((H, B, HEAD), BF),
+            V((H, HEAD, HEAD), F32),
             V((H, HEAD, HEAD), BF),
             V((H, HEAD, HEAD), BF),
             V((H, B, HEAD), F32),
@@ -493,6 +582,8 @@
             V((H, HEAD), F32),
             V((H, HEAD), F32),
             V((H, HEAD), F32),
+            V((G, H, HEAD), F32),
+            V((Z, H, HEAD), F32),
             V((M, H, HEAD), F32),
             V((1, F), BF),
             DMA((NC + 2,)),
@@ -507,8 +598,8 @@
             DMA((1,)),
             DMA((1,)),
             DMA((NC,)),
-            DMA((1,)),
-            DMA((1,)),
+            DMA((3,)),
+            DMA((3,)),
             pltpu.SemaphoreType.REGULAR,
         ],
         compiler_params=pltpu.CompilerParams(

time: 25.5 us -> 24.1 us (0.945)
  Pallas kernels: 24.7 us -> 23.3 us
    pallas_call x1, Pallas kernels: 23.7 us -> 22.3 us  [per_device(): pl.pallas_call(functools.partial(kernel, cfg), out_shape=tuple((V(shape,...]
where the time goes in v2:
time: 24.1 us; the launch traced here: 23.9 us
  Pallas kernels  23.3 us (97%)
  between operations  0.64 us (3%)
    pallas_call x1, Pallas kernels, per_device(): pl.pallas_call(functools.partial(kernel, cfg), out_shape=tuple((V(shape,...  22.3 us
    pallas_call x1, Pallas kernels, per_device(): pl.pallas_call(flush, out_shape=tuple((jax.ShapeDtypeStruct(shape, BF) fo...  1 us

profile of v2, /device:TPU:16, one launch (start us, length us, event | category | flops | bytes accessed | tf_op | source)
XLA Modules:
  0.0 23.9 jit_solution(18019179103719522152)
XLA Ops:
  0.6 22.3 %shard_map.103 = (bf16[512,1024]{1,0:T(8,128)(2,1)S(1)}, bf16[8,8,128]{2,1,0:T(8,128)(2,1)S(1)}, bf16[1,1024]{1,0:T(2,128)(2,1)S(1)}) custom-call(bf16[512,1024]{1,0:T(8,128)(2,1)} %bitcast.4, bf16[1,1024]{1,0:T(2,128)(2,1)} %tok_hbm.1, bf16[2048,1024]{1,0:T(8,128)(2,1)} %wq.1, bf16[2048,1024]{1,0:T(8,128)(2,1)} %wk.1, bf16[2048,1024]{1,0:T(8,128)(2,1)} %wv.1, ...), custom_call_target="tpu_custom_call" | custom-call | tf_op jit(solution)/shard_map/pallas_call | solution.py:548
  22.9 1.0 %shard_map.104 = (bf16[512,1024]{1,0:T(8,128)(2,1)}, bf16[8,8,128]{2,1,0:T(8,128)(2,1)}, bf16[1,1024]{1,0:T(2,128)(2,1)}) custom-call(bf16[512,1024]{1,0:T(8,128)(2,1)S(1)} %get-tuple-element.9.refs_0_, bf16[8,8,128]{2,1,0:T(8,128)(2,1)S(1)} %get-tuple-element.10.refs_1_, bf16[1,1024]{1,0:T(2,128)(2,1)S(1)} %get-tuple-element.11.refs_2_), custom_call_target="tpu_custom_call" | custom-call | tf_op jit(solution)/shard_map/pallas_call | solution.py:609

commit v3 on v2

--- a/solution.py
+++ b/solution.py
@@ -297,10 +297,16 @@
             for hh in range(hc):
                 cache[c * hc + hh] = run[hh * R:(hh + 1) * R].astype(BF)
 
-    def q_project(cs):
+    def q_start(cs):
+        row = (B + PAD) // 16 * 8
+        for c in cs:
+            for at in (slice(0, row), slice(row, B + PAD)):
+                acc[0, c, at, :] = dot(xbuf[me, at, :], wbuf[2, c, 0])
+
+    def q_project(cs, started):
         totals = []
         for c in cs:
-            total = dot(xbuf[me], wbuf[2, c, 0])
+            total = acc[0, c] if c in started else dot(xbuf[me], wbuf[2, c, 0])
             for d in range(1, T):
                 total = total + dot(xbuf[lax.rem(me + d, T)], wbuf[2, c, d])
             totals.append(total)
@@ -427,14 +433,16 @@
             if c > 0:
                 kv_finish(c - 1)
                 kv_send(c - 1)
+    started = list(range(min(1, NC - 1)))
     with jax.named_scope("kvlast"):
+        q_start(started)
         kv_finish(NC - 1)
         kv_send(NC - 1)
     groups = [range(c, min(c + 2, NC)) for c in range(0, NC, 2)]
     ready = 0
     for n, cs in enumerate(groups):
         with jax.named_scope(f"q{n}"):
-            q_project(cs)
+            q_project(cs, started)
         if n < len(groups) - 1:
             for c in cs:
                 attends([c])
@@ -446,16 +454,20 @@
     rest = list(groups[-1])
     step = 0
     if levels > 0:
-        climbs([0], 0)
+        climbs(range(min(1, NC - 1)), 0)
         step = 1
     for c in rest:
         attends([c])
         if levels > 0:
             more = NC if c == rest[-1] else min(step + 1, NC)
-            climbs(range(step, more), 0)
+            climbs(range(step, min(more, NC - 1)), 0)
             step = more
+    if levels > 1:
+        climbs([0], 1)
+    if levels > 0:
+        climbs([NC - 1], 0)
     for level in range(1, levels):
-        climbs(range(NC), level)
+        climbs(range(1 if level == 1 else 0, NC), level)
     with jax.named_scope("w_relay"):
         read_relay()
     middle = Z // 2
@@ -508,9 +520,15 @@
 
 
 def flush(*refs):
-    n = len(refs) // 2
+    n = (len(refs) - 1) // 2
     sems = refs[-1]
-    copies = [pltpu.make_async_copy(refs[i], refs[n + i], sems.at[i]) for i in range(n)]
+    copies = []
+    for i in range(n):
+        rows = refs[i].shape[0]
+        pieces = 4 if i == 0 else 1
+        for k in range(pieces):
+            at = pl.ds(k * (rows // pieces), rows // pieces)
+            copies.append(pltpu.make_async_copy(refs[i].at[at], refs[n + i].at[at], sems.at[len(copies)]))
     for cp in copies:
         cp.start()
     for cp in copies:
@@ -611,7 +629,7 @@
         out_shape=tuple(jax.ShapeDtypeStruct(shape, BF) for shape in shapes),
         in_specs=[vm] * len(shapes),
         out_specs=(any_,) * len(shapes),
-        scratch_shapes=[DMA((len(shapes),))],
+        scratch_shapes=[DMA((len(shapes) + 3,))],
     )(*(pltpu.with_memory_space_constraint(a, V) for a in held))
     return (mixed[None], cache[None], new_read)
 

time: 24.1 us -> 23.9 us (level)
  no operation moved by 1% of the time
where the time goes in v3:
time: 23.9 us; the launch traced here: 23.8 us
  Pallas kernels  23.1 us (97%)
  between operations  0.64 us (3%)
    pallas_call x1, Pallas kernels, per_device(): pl.pallas_call(functools.partial(kernel, cfg), out_shape=tuple((V(shape,...  22.1 us
    pallas_call x1, Pallas kernels, per_device(): pl.pallas_call(flush, out_shape=tuple((jax.ShapeDtypeStruct(shape, BF) fo...  1.02 us

profile of v3, /device:TPU:16, one launch (start us, length us, event | category | flops | bytes accessed | tf_op | source)
XLA Modules:
  0.0 23.8 jit_solution(1471868754848812351)
XLA Ops:
  0.6 22.1 %shard_map.103 = (bf16[512,1024]{1,0:T(8,128)(2,1)S(1)}, bf16[8,8,128]{2,1,0:T(8,128)(2,1)S(1)}, bf16[1,1024]{1,0:T(2,128)(2,1)S(1)}) custom-call(bf16[512,1024]{1,0:T(8,128)(2,1)} %bitcast.4, bf16[1,1024]{1,0:T(2,128)(2,1)} %tok_hbm.1, bf16[2048,1024]{1,0:T(8,128)(2,1)} %wq.1, bf16[2048,1024]{1,0:T(8,128)(2,1)} %wk.1, bf16[2048,1024]{1,0:T(8,128)(2,1)} %wv.1, ...), custom_call_target="tpu_custom_call" | custom-call | tf_op jit(solution)/shard_map/pallas_call | solution.py:566
  22.7 1.0 %shard_map.104 = (bf16[512,1024]{1,0:T(8,128)(2,1)}, bf16[8,8,128]{2,1,0:T(8,128)(2,1)}, bf16[1,1024]{1,0:T(2,128)(2,1)}) custom-call(bf16[512,1024]{1,0:T(8,128)(2,1)S(1)} %get-tuple-element.9.refs_0_, bf16[8,8,128]{2,1,0:T(8,128)(2,1)S(1)} %get-tuple-element.10.refs_1_, bf16[1,1024]{1,0:T(2,128)(2,1)S(1)} %get-tuple-element.11.refs_2_), custom_call_target="tpu_custom_call" | custom-call | tf_op jit(solution)/shard_map/pallas_call | solution.py:627

commit v4 on v3

--- a/solution.py
+++ b/solution.py
@@ -136,10 +136,8 @@
         def _():
             pl.semaphore_signal(up_sem, inc=1, device_id={"sp": t * G + j}, device_id_type=MESH)
 
-    for cs in ([c] for c in range(1, NC // 2)):
-        own_part(cs)
     with jax.named_scope("own_last"):
-        own_part(range(max(NC // 2, 1), NC))
+        own_part(range(1, NC))
 
     ltab.wait()
     top = 2 * B

time: 23.9 us -> 23.9 us (level)
  no operation moved by 1% of the time
where the time goes in v4:
time: 23.9 us; the launch traced here: 23.8 us
  Pallas kernels  23.1 us (97%)
  between operations  0.64 us (3%)
    pallas_call x1, Pallas kernels, per_device(): pl.pallas_call(functools.partial(kernel, cfg), out_shape=tuple((V(shape,...  22.1 us
    pallas_call x1, Pallas kernels, per_device(): pl.pallas_call(flush, out_shape=tuple((jax.ShapeDtypeStruct(shape, BF) fo...  1.02 us

profile of v4, /device:TPU:16, one launch (start us, length us, event | category | flops | bytes accessed | tf_op | source)
XLA Modules:
  0.0 23.8 jit_solution(18358385466840757317)
XLA Ops:
  0.6 22.1 %shard_map.103 = (bf16[512,1024]{1,0:T(8,128)(2,1)S(1)}, bf16[8,8,128]{2,1,0:T(8,128)(2,1)S(1)}, bf16[1,1024]{1,0:T(2,128)(2,1)S(1)}) custom-call(bf16[512,1024]{1,0:T(8,128)(2,1)} %bitcast.4, bf16[1,1024]{1,0:T(2,128)(2,1)} %tok_hbm.1, bf16[2048,1024]{1,0:T(8,128)(2,1)} %wq.1, bf16[2048,1024]{1,0:T(8,128)(2,1)} %wk.1, bf16[2048,1024]{1,0:T(8,128)(2,1)} %wv.1, ...), custom_call_target="tpu_custom_call" | custom-call | tf_op jit(solution)/shard_map/pallas_call | solution.py:564
  22.8 1.0 %shard_map.104 = (bf16[512,1024]{1,0:T(8,128)(2,1)}, bf16[8,8,128]{2,1,0:T(8,128)(2,1)}, bf16[1,1024]{1,0:T(2,128)(2,1)}) custom-call(bf16[512,1024]{1,0:T(8,128)(2,1)S(1)} %get-tuple-element.9.refs_0_, bf16[8,8,128]{2,1,0:T(8,128)(2,1)S(1)} %get-tuple-element.10.refs_1_, bf16[1,1024]{1,0:T(2,128)(2,1)S(1)} %get-tuple-element.11.refs_2_), custom_call_target="tpu_custom_call" | custom-call | tf_op jit(solution)/shard_map/pallas_call | solution.py:625
